TPU v7x, 32 devices: a whole 2x2x4 slice. The times are simulated.
32 devices in a mesh: grp: 2 (over y), sp: 4 (over z), tp: 4 (over x, core).
Axes of the slice: x: 2, y: 2, z: 4, core: 2. Of those that a mesh axis runs over, the one named last changes fastest.
Arguments:
- prompt_rows: bfloat16 [6144, 2048], P(('grp', 'sp')), parts along dimension 0, may hold values from -6 to 6
- norm_gain: float32 [2048], replicated, may hold values from 0.1 to 1.9
- key_weight: bfloat16 [2048, 1024], P(None, 'tp'), may hold values from -0.125 to 0.125
- value_weight: bfloat16 [2048, 1024], P(None, 'tp'), may hold values from -0.125 to 0.125
- new_query: bfloat16 [2048], P(('grp', 'tp')), parts along dimension 0, may hold values from -6 to 6
- score_offset: float32 [16], P('tp'), may hold values from -11.5 to -4
- output_gain: float32 [1024], P('tp'), may hold values from 0.1 to 1.9
Outputs:
- key_cache: bfloat16 [8, 4, 4, 768, 64], P(('grp', 'tp'), 'sp'), parts along dimension 0
- value_cache: bfloat16 [8, 4, 4, 768, 64], P(('grp', 'tp'), 'sp'), parts along dimension 0
- first_read: bfloat16 [2048], P(('grp', 'tp')), parts along dimension 0
There are 2 independent parts, one for each index of `grp`. A program takes and returns all parts, laid end to end along the dimension named above; an argument that names none is the same for every part. Nothing has to cross between parts.
All inputs are finite; a program needn't handle non-finite values.
Results may differ from a plain program's by a relative error of at most 0.0059.
Values may be sent and summed in bfloat16 or wider, within the bound.
A program may use at most 64 MiB of HBM per device.

v0:
```python
import jax
import jax.numpy as jnp
from jax import lax
from jax.sharding import PartitionSpec as P

EPSILON = 1e-06


def prefix(value, axis, combine, identity):
    peers, position = (lax.axis_size(axis), lax.axis_index(axis))
    everything = lax.all_gather(value, axis)
    start = jnp.broadcast_to(jnp.asarray(identity, value.dtype), value.shape)

    def hop(k, before):
        at = peers - 1 - k
        reached = at > position
        new = combine(before, everything[at])
        return jnp.where(reached, new, before)

    return lax.fori_loop(0, peers, hop, start)


def normalize(rows, norm_gain):
    rows32 = rows.astype(jnp.float32)
    mean_square = jnp.mean(rows32 * rows32, axis=-1, keepdims=True)
    return (rows32 * lax.rsqrt(mean_square + EPSILON) * norm_gain).astype(jnp.bfloat16)


def project_rows(rows, norm_gain, key_weight, value_weight):
    normed = normalize(rows, norm_gain)
    keys = jnp.dot(normed, key_weight, preferred_element_type=jnp.float32).astype(jnp.bfloat16)
    values = jnp.dot(normed, value_weight, preferred_element_type=jnp.float32).astype(jnp.bfloat16)
    return (keys, values)


def cache_layout(keys, values, head_count):
    devices = lax.axis_size("sp")
    subs = devices // head_count
    depth = keys.shape[1] // head_count
    rows = keys.shape[0] // subs

    def arrange(cache):
        split = cache.reshape(subs, rows, head_count, depth)
        return jnp.transpose(split, (2, 0, 1, 3)).reshape(devices, 1, rows, depth)

    moved_keys, moved_values = (
        lax.all_to_all(arrange(keys), "sp", split_axis=0, concat_axis=1, tiled=True),
        lax.all_to_all(arrange(values), "sp", split_axis=0, concat_axis=1, tiled=True),
    )
    target = (1, 1, devices, rows, depth)
    return (moved_keys.reshape(target), moved_values.reshape(target))


def add_terms(first_part, second_part):
    return first_part + second_part


def read_early(new_query, keys, values, score_offset):
    head_count = score_offset.shape[0]
    depth = keys.shape[1] // head_count
    query2 = new_query.reshape(head_count, depth)
    keys3 = keys.reshape(keys.shape[0], head_count, depth)
    scores = jnp.einsum("hd,shd->hs", query2, keys3, preferred_element_type=jnp.float32)
    scores = scores * depth ** (-0.5) + score_offset[:, None]
    remain = jax.nn.log_sigmoid(-scores)
    within = lax.cumsum(remain, axis=1, reverse=True) - remain
    totals = jnp.sum(remain, axis=1)
    beyond = prefix(totals, "sp", add_terms, jnp.zeros_like(totals))
    sticks = jnp.exp(jax.nn.log_sigmoid(scores) + within + beyond[:, None]).astype(jnp.bfloat16)
    values3 = values.reshape(values.shape[0], head_count, depth)
    partial_value = jnp.einsum("hs,shd->hd", sticks, values3, preferred_element_type=jnp.float32)
    return lax.psum(partial_value, "sp")


def finish_read(mixed, output_gain, head_count):
    spread = jnp.mean(mixed * mixed, axis=-1, keepdims=True)
    result = mixed * lax.rsqrt(spread + EPSILON) * output_gain.reshape(head_count, -1)
    return result.reshape(-1).astype(jnp.bfloat16)


def body(prompt_rows, norm_gain, key_weight, value_weight, new_query, score_offset, output_gain):
    head_count = score_offset.shape[0]
    keys_here, values_here = project_rows(prompt_rows, norm_gain, key_weight, value_weight)
    keys_all, values_all = cache_layout(keys_here, values_here, head_count)
    local_keys, local_values = project_rows(prompt_rows, norm_gain, key_weight, value_weight)
    mixed = read_early(new_query, local_keys, local_values, score_offset)
    return (keys_all, values_all, finish_read(mixed, output_gain, head_count))


def solution(mesh):
    in_specs = (
        P(("grp", "sp"), None),
        P(),
        P(None, "tp"),
        P(None, "tp"),
        P(("grp", "tp")),
        P("tp"),
        P("tp"),
    )
    out_specs = (
        P(("grp", "tp"), "sp", None, None, None),
        P(("grp", "tp"), "sp", None, None, None),
        P(("grp", "tp")),
    )
    return jax.shard_map(body, mesh=mesh, in_specs=in_specs, out_specs=out_specs, check_vma=False)
```

profile of v0, /device:TPU:0, one launch (start us, length us, event | category | flops | bytes accessed | tf_op | source)
XLA Modules:
  0.0 56.2 jit_solution(451119704450405001)
XLA Ops:
  0.6 0.0 copy-start
  0.6 0.0 copy-start.1
  0.7 2.7 %fusion = f32[768]{0:T(1024)S(1)} fusion(bf16[768,2048]{1,0:T(8,128)(2,1)} %param.9), kind=kLoop, calls=%fused_computation.4 | loop fusion | flops 4717824 | bytes 3148800 | tf_op jit(solution)/shard_map/reduce_sum | solution.py:25
  3.4 0.4 copy-done.1
  3.8 0.0 copy-start.5
  3.8 2.1 %convolution_convert_fusion.1 = bf16[768,256]{0,1:T(8,128)(2,1)} fusion(bf16[2048,256]{1,0:T(8,128)(2,1)S(1)} %copy-done, bf16[768,2048]{1,0:T(8,128)(2,1)S(1)} %copy-done.1, f32[2048]{0:T(1024)S(1)} %copy-done.6, f32[768]{0:T(1024)S(1)} %add_rsqrt_fusion), kind=kOutput, calls=%fused_computation.8 | convolution fusion | flops 811794432 | bytes 4598784 | tf_op jit(solution)/shard_map/dot_general | solution.py:31
  5.9 6.3 %all-to-all-start = ((bf16[4,1,768,64]{2,3,1,0:T(8,128)(2,1)}), bf16[4,1,768,64]{2,3,1,0:T(8,128)(2,1)S(1)}, u32[]{:S(2)}, u32[]{:S(2)}) async-start(bf16[4,1,768,64]{2,3,1,0:T(8,128)(2,1)} %bitcast.2), calls=%async_computation | async-start | bytes 786432 | tf_op jit(solution)/shard_map/all_to_all | solution.py:47
  12.3 0.1 reshape.98
  12.4 1.2 %fusion.16 = f32[4,1,768]{2,1,0:T(1,128)S(1)} fusion(bf16[768,4,64]{0,2,1:T(8,128)(2,1)} %bitcast.8, bf16[4,64,1]{1,2,0:T(2,128)(2,1)S(1)} %reshape.98), kind=kOutput, calls=%fused_computation.31 | convolution fusion | flops 393216 | bytes 406016 | tf_op jit(solution)/shard_map/hd,shd->hs/dot_general | solution.py:63
  13.5 0.2 fusion.15
  13.7 5.0 %reduce-window.6 = f32[4,6,128]{2,1,0:T(8,128)S(1)} reduce-window(f32[4,6,128]{2,1,0:T(8,128)S(1)} %reshape.83, f32[]{:T(128)} %constant.61.clone.1), window={size=1x1x128 pad=0_0x0_0x0_127}, to_apply=%region_1.0 | reduce-window | flops 390144 | bytes 24580 | tf_op jit(solution)/shard_map/reduce-window
  18.7 0.1 slice_reduce_fusion
  18.8 0.2 reduce-window.9
  19.0 0.1 slice.7
  19.1 0.1 add_bitcast_fusion
  19.1 0.6 %dynamic-slice = u32[1]{0:T(128)} dynamic-slice(u32[32]{0:T(128)S(1)} %copy-done.7, u32[]{:T(128)S(6)} %add.95), dynamic_slice_sizes={1} | dynamic-slice | bytes 12
  20.4 0.1 negate_dynamic-update-slice_fusion
  20.5 12.2 %all-reduce = f32[16]{0:T(128)S(1)} all-reduce(f32[16]{0:T(128)S(1)} %negate_dynamic-update-slice_fusion), channel_id=2, replica_groups=mesh['grp'=2,'sp'=4,'tp'=4] {'sp'}, use_global_device_ids=true, to_apply=%add | all-reduce | flops 16 | bytes 128
  32.6 0.1 reshape.87
  32.7 0.1 while.16
  32.9 0.1 fusion.13
  33.0 0.0 copy-start.3
  33.0 3.9 %convolution_convert_fusion = bf16[768,256]{0,1:T(8,128)(2,1)} fusion(bf16[2048,256]{1,0:T(8,128)(2,1)S(1)} %copy-done.5, bf16[768,2048]{1,0:T(8,128)(2,1)} %param.9, f32[2048]{0:T(1024)S(1)} %copy-done.6, f32[768]{0:T(1024)S(1)} %add_rsqrt_fusion), kind=kOutput, calls=%fused_computation.7 | convolution fusion | flops 811794432 | bytes 4598784 | tf_op jit(solution)/shard_map/dot_general | solution.py:32
  36.9 3.5 %all-to-all-start.1 = ((bf16[4,1,768,64]{2,3,1,0:T(8,128)(2,1)}), bf16[4,1,768,64]{2,3,1,0:T(8,128)(2,1)S(1)}, u32[]{:S(2)}, u32[]{:S(2)}) async-start(bf16[4,1,768,64]{2,3,1,0:T(8,128)(2,1)} %bitcast.6), calls=%async_computation.1 | async-start | bytes 786432 | tf_op jit(solution)/shard_map/all_to_all | solution.py:48
  40.4 1.2 %fusion.11 = f32[4,1,64]{2,1,0:T(1,128)S(1)} fusion(bf16[768,4,64]{0,2,1:T(8,128)(2,1)} %bitcast.12, bf16[4,768,1]{1,0,2:T(4,128)(2,1)S(1)} %fusion.13), kind=kOutput, calls=%fused_computation.21 | convolution fusion | flops 393216 | bytes 400384 | tf_op jit(solution)/shard_map/hs,shd->hd/dot_general | solution.py:71
  41.6 0.1 reshape.86
  41.7 12.1 %psum.7 = f32[4,64]{1,0:T(4,128)S(1)} all-reduce(f32[4,64]{1,0:T(4,128)S(1)} %bitcast.54), channel_id=1, replica_groups=mesh['grp'=2,'sp'=4,'tp'=4] {'sp'}, use_global_device_ids=true, to_apply=%region_6.7 | all-reduce | flops 256 | bytes 2048 | tf_op jit(solution)/shard_map/psum | solution.py:72
  53.9 0.1 multiply_reduce_fusion
  54.0 0.1 multiply_convert_fusion
  54.1 0.6 %convert_element_type.31 = bf16[256]{0:T(256)(128)(2,1)} reshape(bf16[4,64]{1,0:T(4,128)(2,1)S(1)} %multiply_convert_fusion) | data formatting | bytes 1024 | tf_op jit(solution)/shard_map/convert_element_type | solution.py:78
  54.7 0.7 %copy.46 = bf16[1,1,4,768,64]{3,4,2,1,0:T(8,128)(2,1)} copy(bf16[1,1,4,768,64]{3,4,2,1,0:T(8,128)(2,1)S(1)} %bitcast.52) | data formatting | bytes 786432
  55.4 0.7 %copy.47 = bf16[1,1,4,768,64]{3,4,2,1,0:T(8,128)(2,1)} copy(bf16[1,1,4,768,64]{3,4,2,1,0:T(8,128)(2,1)S(1)} %bitcast.53) | data formatting | bytes 786432
  (22 shorter events, 0.1 us)
Async XLA Ops:
  0.6 2.8 %copy-start = (bf16[2048,256]{1,0:T(8,128)(2,1)S(1)}, bf16[2048,256]{1,0:T(8,128)(2,1)}, u32[]{:S(2)}) copy-start(bf16[2048,256]{1,0:T(8,128)(2,1)} %param.11) | copy-start | bytes 3145732
  0.6 3.2 %copy-start.1 = (bf16[768,2048]{1,0:T(8,128)(2,1)S(1)}, bf16[768,2048]{1,0:T(8,128)(2,1)}, u32[]{:S(2)}) copy-start(bf16[768,2048]{1,0:T(8,128)(2,1)} %param.9) | copy-start | bytes 9437188
  0.7 3.1 %copy-start.6 = (f32[2048]{0:T(1024)S(1)}, f32[2048]{0:T(1024)}, u32[]{:S(2)}) copy-start(f32[2048]{0:T(1024)} %param.10) | copy-start | bytes 24580
  3.8 8.5 %copy-start.4 = (bf16[256]{0:T(256)(128)(2,1)S(1)}, bf16[256]{0:T(256)(128)(2,1)}, u32[]{:S(2)}) copy-start(bf16[256]{0:T(256)(128)(2,1)} %param.13) | copy-start | bytes 1540
  3.8 9.7 %copy-start.2 = (f32[4]{0:T(128)S(1)}, f32[4]{0:T(128)}, u32[]{:S(2)}) copy-start(f32[4]{0:T(128)} %param.14) | copy-start | bytes 52
  3.8 15.3 %copy-start.7 = (u32[32]{0:T(128)S(1)}, u32[32]{0:T(128)}, u32[]{:S(2)}) copy-start(u32[32]{0:T(128)} %constant.71) | copy-start | bytes 388
  3.8 29.2 %copy-start.5 = (bf16[2048,256]{1,0:T(8,128)(2,1)S(1)}, bf16[2048,256]{1,0:T(8,128)(2,1)}, u32[]{:S(2)}) copy-start(bf16[2048,256]{1,0:T(8,128)(2,1)} %param.12) | copy-start | bytes 3145732
  5.9 31.0 %all-to-all-start = ((bf16[4,1,768,64]{2,3,1,0:T(8,128)(2,1)}), bf16[4,1,768,64]{2,3,1,0:T(8,128)(2,1)S(1)}, u32[]{:S(2)}, u32[]{:S(2)}) async-start(bf16[4,1,768,64]{2,3,1,0:T(8,128)(2,1)} %bitcast.2), calls=%async_computation | async-start | bytes 786432 | tf_op jit(solution)/shard_map/all_to_all | solution.py:47
  33.0 8.6 %copy-start.3 = (f32[256]{0:T(256)S(1)}, f32[256]{0:T(256)}, u32[]{:S(2)}) copy-start(f32[256]{0:T(256)} %param.15) | copy-start | bytes 3076
  36.9 17.7 %all-to-all-start.1 = ((bf16[4,1,768,64]{2,3,1,0:T(8,128)(2,1)}), bf16[4,1,768,64]{2,3,1,0:T(8,128)(2,1)S(1)}, u32[]{:S(2)}, u32[]{:S(2)}) async-start(bf16[4,1,768,64]{2,3,1,0:T(8,128)(2,1)} %bitcast.6), calls=%async_computation.1 | async-start | bytes 786432 | tf_op jit(solution)/shard_map/all_to_all | solution.py:48
where the time goes:
time: 56.6 us; the launch traced here: 56.2 us
  blocking collectives  24.3 us (43%)
  starting transfers between devices  9.81 us (17%)
  other arithmetic  8.65 us (15%)
  matrix products  8.39 us (15%)
  local copies, waits for them, and re-layouts  3.53 us (6%)
  between operations  1.39 us (2%)
    unnamed x1, blocking collectives  12.2 us
    psum x1, blocking collectives, read_early(): return lax.psum(partial_value, 'sp')  12.1 us
    all_to_all x1, starting transfers between devices, cache_layout(): lax.all_to_all(arrange(keys), 'sp', split_axis=0, concat_axis=1, tiled=True)  6.35 us
    another operation x2, other arithmetic  5.16 us
    dot_general x1, matrix products, project_rows(): jnp.dot(normed, value_weight, preferred_element_type=jnp.float32)  3.9 us
    all_to_all x1, starting transfers between devices, cache_layout(): lax.all_to_all(arrange(values), 'sp', split_axis=0, concat_axis=1, tiled=...  3.46 us
    reduce_sum x1, other arithmetic, normalize(): mean_square = jnp.mean(rows32 * rows32, axis=-1, keepdims=True)  2.72 us
    unnamed x20, local copies, waits for them, and re-layouts  2.51 us
  transfers between devices with their start and end apart: 2, of which 0 were waited for; matrix products, arithmetic and copies ran while one was open for 25% of the time, Pallas kernels for 0%

commit v1 on v0

--- a/solution.py
+++ b/solution.py
@@ -4,6 +4,7 @@
 from jax.sharding import PartitionSpec as P
 
 EPSILON = 1e-06
+sectors_measure = lambda xs: jnp.sum(lax.all_gather(xs, axis_name="sp"), axis=0)
 
 
 def prefix(value, axis, combine, identity):
@@ -69,7 +70,7 @@
     sticks = jnp.exp(jax.nn.log_sigmoid(scores) + within + beyond[:, None]).astype(jnp.bfloat16)
     values3 = values.reshape(values.shape[0], head_count, depth)
     partial_value = jnp.einsum("hs,shd->hd", sticks, values3, preferred_element_type=jnp.float32)
-    return lax.psum(partial_value, "sp")
+    return sectors_measure(partial_value)
 
 
 def finish_read(mixed, output_gain, head_count):

time: 56.6 us -> 64.5 us (1.14)
  waiting for transfers between devices: 0.01 us -> 8.16 us
    psum x1 -> x0, blocking collectives: 12.1 us -> none  [read_early(): return lax.psum(partial_value, 'sp')]
    all_gather x0 -> x1, blocking collectives: none -> 11.9 us  [lax.all_gather(xs, axis_name='sp')]
    all_to_all x1, waiting for transfers between devices: 0.01 us -> 8.16 us  [cache_layout(): lax.all_to_all(arrange(values), 'sp', split_axis=0, concat_axis=1, tiled=...]
  transfers between devices with their start and end apart: 2 -> 2, of which waited for: 0 -> 1; matrix products, arithmetic and copies ran while one was open for 25% -> 21% of each run, Pallas kernels for 0% -> 0%
where the time goes in v1:
time: 64.5 us; the launch traced here: 64.1 us
  blocking collectives  24.1 us (37%)
  starting transfers between devices  9.82 us (15%)
  other arithmetic  9.17 us (14%)
  matrix products  8.41 us (13%)
  waiting for transfers between devices  8.16 us (13%)
  local copies, waits for them, and re-layouts  2.93 us (5%)
  between operations  1.4 us (2%)
    unnamed x1, blocking collectives  12.2 us
    all_gather x1, blocking collectives, lax.all_gather(xs, axis_name='sp')  11.9 us
    all_to_all x1, waiting for transfers between devices, cache_layout(): lax.all_to_all(arrange(values), 'sp', split_axis=0, concat_axis=1, tiled=...  8.16 us
    all_to_all x1, starting transfers between devices, cache_layout(): lax.all_to_all(arrange(keys), 'sp', split_axis=0, concat_axis=1, tiled=True)  6.35 us
    another operation x2, other arithmetic  5.16 us
    dot_general x1, matrix products, project_rows(): jnp.dot(normed, value_weight, preferred_element_type=jnp.float32)  3.95 us
    all_to_all x1, starting transfers between devices, cache_layout(): lax.all_to_all(arrange(values), 'sp', split_axis=0, concat_axis=1, tiled=...  3.47 us
    reduce_sum x1, other arithmetic, normalize(): mean_square = jnp.mean(rows32 * rows32, axis=-1, keepdims=True)  2.72 us
  transfers between devices with their start and end apart: 2, of which 1 were waited for; matrix products, arithmetic and copies ran while one was open for 21% of the time, Pallas kernels for 0%

profile of v1, /device:TPU:0, one launch (start us, length us, event | category | flops | bytes accessed | tf_op | source)
XLA Modules:
  0.0 64.1 jit_solution(161544141357022260)
XLA Ops:
  0.6 0.0 copy-start
  0.6 0.0 copy-start.1
  0.7 2.7 %fusion = f32[768]{0:T(1024)S(1)} fusion(bf16[768,2048]{1,0:T(8,128)(2,1)} %param.9), kind=kLoop, calls=%fused_computation.4 | loop fusion | flops 4717824 | bytes 3148800 | tf_op jit(solution)/shard_map/reduce_sum | solution.py:26
  3.4 0.4 copy-done.1
  3.8 0.0 copy-start.5
  3.8 2.1 %convolution_convert_fusion.1 = bf16[768,256]{0,1:T(8,128)(2,1)} fusion(bf16[2048,256]{1,0:T(8,128)(2,1)S(1)} %copy-done, bf16[768,2048]{1,0:T(8,128)(2,1)S(1)} %copy-done.1, f32[2048]{0:T(1024)S(1)} %copy-done.6, f32[768]{0:T(1024)S(1)} %add_rsqrt_fusion), kind=kOutput, calls=%fused_computation.8 | convolution fusion | flops 811794432 | bytes 4598784 | tf_op jit(solution)/shard_map/dot_general | solution.py:32
  5.9 6.3 %all-to-all-start = ((bf16[4,1,768,64]{2,3,1,0:T(8,128)(2,1)}), bf16[4,1,768,64]{2,3,1,0:T(8,128)(2,1)S(1)}, u32[]{:S(2)}, u32[]{:S(2)}) async-start(bf16[4,1,768,64]{2,3,1,0:T(8,128)(2,1)} %bitcast.2), calls=%async_computation | async-start | bytes 786432 | tf_op jit(solution)/shard_map/all_to_all | solution.py:48
  12.3 0.1 reshape.101
  12.4 1.2 %fusion.16 = f32[4,1,768]{2,1,0:T(1,128)S(1)} fusion(bf16[768,4,64]{0,2,1:T(8,128)(2,1)} %bitcast.8, bf16[4,64,1]{1,2,0:T(2,128)(2,1)S(1)} %reshape.101), kind=kOutput, calls=%fused_computation.32 | convolution fusion | flops 393216 | bytes 406016 | tf_op jit(solution)/shard_map/hd,shd->hs/dot_general | solution.py:64
  13.5 0.2 fusion.15
  13.7 5.0 %reduce-window.6 = f32[4,6,128]{2,1,0:T(8,128)S(1)} reduce-window(f32[4,6,128]{2,1,0:T(8,128)S(1)} %reshape.83, f32[]{:T(128)} %constant.61.clone.1), window={size=1x1x128 pad=0_0x0_0x0_127}, to_apply=%region_1.0 | reduce-window | flops 390144 | bytes 24580 | tf_op jit(solution)/shard_map/reduce-window
  18.7 0.1 slice_reduce_fusion
  18.8 0.2 reduce-window.9
  19.0 0.1 slice.7
  19.1 0.6 dynamic-slice
  20.3 0.1 negate_dynamic-update-slice_fusion
  20.4 12.2 %all-reduce = f32[16]{0:T(128)S(1)} all-reduce(f32[16]{0:T(128)S(1)} %negate_dynamic-update-slice_fusion), channel_id=2, replica_groups=mesh['grp'=2,'sp'=4,'tp'=4] {'sp'}, use_global_device_ids=true, to_apply=%add | all-reduce | flops 16 | bytes 128
  32.6 0.1 reshape.86
  32.7 0.1 while.16
  32.8 3.9 %convolution_convert_fusion = bf16[768,256]{0,1:T(8,128)(2,1)} fusion(bf16[2048,256]{1,0:T(8,128)(2,1)S(1)} %copy-done.5, bf16[768,2048]{1,0:T(8,128)(2,1)} %param.9, f32[2048]{0:T(1024)S(1)} %copy-done.6, f32[768]{0:T(1024)S(1)} %add_rsqrt_fusion), kind=kOutput, calls=%fused_computation.7 | convolution fusion | flops 811794432 | bytes 4598784 | tf_op jit(solution)/shard_map/dot_general | solution.py:33
  36.8 0.1 add_bitcast_fusion
  36.9 0.1 fusion.13
  37.0 1.2 %fusion.11 = f32[4,1,64]{2,1,0:T(1,128)S(1)} fusion(bf16[768,4,64]{0,2,1:T(8,128)(2,1)} %bitcast.12, bf16[4,768,1]{1,0,2:T(4,128)(2,1)S(1)} %fusion.13), kind=kOutput, calls=%fused_computation.21 | convolution fusion | flops 393216 | bytes 400384 | tf_op jit(solution)/shard_map/hs,shd->hd/dot_general | solution.py:72
  38.2 11.9 %all-gather.2 = f32[4,4,64]{2,1,0:T(4,128)S(1)} all-gather(f32[1,4,64]{2,1,0:T(4,128)S(1)} %bitcast.55), channel_id=3, replica_groups=mesh['grp'=2,'sp'=4,'tp'=4] {'sp'}, dimensions={0}, use_global_device_ids=true | all-gather | bytes 5120 | tf_op jit(solution)/shard_map/all_gather | solution.py:7
  50.1 0.1 multiply_reduce_fusion
  50.3 3.5 %all-to-all-start.1 = ((bf16[4,1,768,64]{2,3,1,0:T(8,128)(2,1)}), bf16[4,1,768,64]{2,3,1,0:T(8,128)(2,1)S(1)}, u32[]{:S(2)}, u32[]{:S(2)}) async-start(bf16[4,1,768,64]{2,3,1,0:T(8,128)(2,1)} %bitcast.6), calls=%async_computation.1 | async-start | bytes 786432 | tf_op jit(solution)/shard_map/all_to_all | solution.py:49
  53.7 0.1 broadcast_multiply_fusion
  53.8 0.1 mul.63
  53.9 0.5 multiply_convert_fusion
  54.4 8.2 %all-to-all-done.1 = bf16[4,1,768,64]{2,3,1,0:T(8,128)(2,1)S(1)} async-done(((bf16[4,1,768,64]{2,3,1,0:T(8,128)(2,1)}), bf16[4,1,768,64]{2,3,1,0:T(8,128)(2,1)S(1)}, u32[]{:S(2)}, u32[]{:S(2)}) %all-to-all-start.1) | async-done | bytes 393248 | tf_op jit(solution)/shard_map/all_to_all | solution.py:49
  62.6 0.7 %copy.46 = bf16[1,1,4,768,64]{3,4,2,1,0:T(8,128)(2,1)} copy(bf16[1,1,4,768,64]{3,4,2,1,0:T(8,128)(2,1)S(1)} %bitcast.53) | data formatting | bytes 786432
  63.3 0.7 %copy.47 = bf16[1,1,4,768,64]{3,4,2,1,0:T(8,128)(2,1)} copy(bf16[1,1,4,768,64]{3,4,2,1,0:T(8,128)(2,1)S(1)} %bitcast.54) | data formatting | bytes 786432
  (23 shorter events, 0.1 us)
Async XLA Ops:
  0.6 2.8 %copy-start = (bf16[2048,256]{1,0:T(8,128)(2,1)S(1)}, bf16[2048,256]{1,0:T(8,128)(2,1)}, u32[]{:S(2)}) copy-start(bf16[2048,256]{1,0:T(8,128)(2,1)} %param.11) | copy-start | bytes 3145732
  0.6 3.2 %copy-start.1 = (bf16[768,2048]{1,0:T(8,128)(2,1)S(1)}, bf16[768,2048]{1,0:T(8,128)(2,1)}, u32[]{:S(2)}) copy-start(bf16[768,2048]{1,0:T(8,128)(2,1)} %param.9) | copy-start | bytes 9437188
  0.7 3.1 %copy-start.6 = (f32[2048]{0:T(1024)S(1)}, f32[2048]{0:T(1024)}, u32[]{:S(2)}) copy-start(f32[2048]{0:T(1024)} %param.10) | copy-start | bytes 24580
  3.8 8.5 %copy-start.4 = (bf16[256]{0:T(256)(128)(2,1)S(1)}, bf16[256]{0:T(256)(128)(2,1)}, u32[]{:S(2)}) copy-start(bf16[256]{0:T(256)(128)(2,1)} %param.13) | copy-start | bytes 1540
  3.8 9.7 %copy-start.2 = (f32[4]{0:T(128)S(1)}, f32[4]{0:T(128)}, u32[]{:S(2)}) copy-start(f32[4]{0:T(128)} %param.14) | copy-start | bytes 52
  3.8 15.3 %copy-start.7 = (u32[32]{0:T(128)S(1)}, u32[32]{0:T(128)}, u32[]{:S(2)}) copy-start(u32[32]{0:T(128)} %constant.71) | copy-start | bytes 388
  3.8 29.0 %copy-start.5 = (bf16[2048,256]{1,0:T(8,128)(2,1)S(1)}, bf16[2048,256]{1,0:T(8,128)(2,1)}, u32[]{:S(2)}) copy-start(bf16[2048,256]{1,0:T(8,128)(2,1)} %param.12) | copy-start | bytes 3145732
  5.9 44.3 %all-to-all-start = ((bf16[4,1,768,64]{2,3,1,0:T(8,128)(2,1)}), bf16[4,1,768,64]{2,3,1,0:T(8,128)(2,1)S(1)}, u32[]{:S(2)}, u32[]{:S(2)}) async-start(bf16[4,1,768,64]{2,3,1,0:T(8,128)(2,1)} %bitcast.2), calls=%async_computation | async-start | bytes 786432 | tf_op jit(solution)/shard_map/all_to_all | solution.py:48
  32.8 21.1 %copy-start.3 = (f32[256]{0:T(256)S(1)}, f32[256]{0:T(256)}, u32[]{:S(2)}) copy-start(f32[256]{0:T(256)} %param.15) | copy-start | bytes 3076
  50.3 12.3 %all-to-all-start.1 = ((bf16[4,1,768,64]{2,3,1,0:T(8,128)(2,1)}), bf16[4,1,768,64]{2,3,1,0:T(8,128)(2,1)S(1)}, u32[]{:S(2)}, u32[]{:S(2)}) async-start(bf16[4,1,768,64]{2,3,1,0:T(8,128)(2,1)} %bitcast.6), calls=%async_computation.1 | async-start | bytes 786432 | tf_op jit(solution)/shard_map/all_to_all | solution.py:49
